TPU v7x, 32 devices: a whole 2x2x4 slice. The times are simulated.
32 devices in a mesh: fs: 8 (over z, x), tp: 4 (over y, core).
Axes of the slice: x: 2, y: 2, z: 4, core: 2. Of those that a mesh axis runs over, the one named last changes fastest.
Arguments:
- query_rows: bfloat16 [16384, 2048], P('fs', 'tp'), may hold values from -16 to 16
- key_rows: bfloat16 [16384, 2048], P('fs', 'tp'), may hold values from -8 to 8
- value_rows: bfloat16 [16384, 2048], P('fs', 'tp'), may hold values from -6 to 6
- mix_lambda: float32 [16], P('tp'), may hold values from 0.3 to 0.8
- head_gain: float32 [128], replicated, may hold values from 0.1 to 1.9
- out_cotangent: bfloat16 [16384, 2048], P('fs'), may hold values from -0.049804688 to 0.049804688
- layer_input: bfloat16 [16384, 2048], P('fs'), may hold values from -6 to 6
- value_cotangent: bfloat16 [16384, 2048], P('fs', 'tp'), may hold values from -0.049804688 to 0.049804688
- out_weight: float32 [2048, 2048], P('tp', 'fs'), may hold values from -0.125 to 0.125
- value_weight: float32 [2048, 2048], P('fs', 'tp'), may hold values from -0.125 to 0.125
- out_basis: bfloat16 [2048, 256], replicated, may hold values from -0.125 to 0.125
- value_basis: bfloat16 [2048, 256], replicated, may hold values from -0.125 to 0.125
- out_first: float32 [256, 2048], P('fs', 'tp'), may hold values from -20 to 20
- out_second: float32 [256, 2048], P('fs', 'tp'), may hold values from 0.02 to 0.5
- value_first: float32 [256, 2048], P('fs', 'tp'), may hold values from -20 to 20
- value_second: float32 [256, 2048], P('fs', 'tp'), may hold values from 0.02 to 0.5
Outputs:
- out_step: float32 [2048, 2048], P('tp', 'fs')
- value_step: float32 [2048, 2048], P('fs', 'tp')
- new_out_weight: float32 [2048, 2048], P('tp', 'fs')
- new_value_weight: float32 [2048, 2048], P('fs', 'tp')
- out_copy: bfloat16 [2048, 2048], P('tp')
- value_copy: bfloat16 [2048, 2048], P(None, 'tp')
- new_out_first: float32 [256, 2048], P('fs', 'tp')
- new_out_second: float32 [256, 2048], P('fs', 'tp')
- new_value_first: float32 [256, 2048], P('fs', 'tp')
- new_value_second: float32 [256, 2048], P('fs', 'tp')
All inputs are finite; a program needn't handle non-finite values.
Results may differ from a plain program's by a relative error of at most 0.001.
Values may be sent and summed in bfloat16 or wider, within the bound.
A program may use at most 192 MiB of HBM per device.

v0:
```python
import functools
import math

import jax
import jax.numpy as jnp
from jax import lax
from jax.experimental import pallas as pl
from jax.experimental.pallas import tpu as pltpu
from jax.sharding import PartitionSpec as P

DH = 64
DV = 128


EPSILON_NORM = 1e-05
EPSILON_ADAM = 1e-08
BETA_ONE = 0.9
BETA_TWO = 0.95
CLIP_RMS = 1.0
LEARN_RATE = 0.01
TILE = 256
F32 = jnp.float32
BF16 = jnp.bfloat16


def dot_f32(left, right, dims=((1,), (0,))):
    return lax.dot_general(left, right, (dims, ((), ())), preferred_element_type=F32)


def split_two(wide):
    high = wide.astype(BF16)
    return high, (wide - high.astype(F32)).astype(BF16)


def fold_rows(tile, op):
    rows, cols = tile.shape
    return op(tile.reshape(rows // 8, 8, cols), axis=0)


def grads_kernel(
    lam_ref, query_ref, key_ref, value_ref, gain_ref, cot_ref, input_ref, vcot_ref,
    obasis_ref, vbasis_ref, oproj_ref, vproj_ref,
    score_one, score_two, mix_ref, value_t, obasis_t, vbasis_t, cb_high, cb_low,
):
    block = pl.program_id(0)
    head = pl.program_id(1)
    span = query_ref.shape[0]
    seq_len = key_ref.shape[0]

    @pl.when((block == 0) & (head == 0))
    def _():
        obasis_t[...] = obasis_ref[...].T
        vbasis_t[...] = vbasis_ref[...].T
        oproj_ref[...] = jnp.zeros_like(oproj_ref)
        vproj_ref[...] = jnp.zeros_like(vproj_ref)

    @pl.when(block == 0)
    def _():
        value_t[head] = value_ref[:, pl.ds(pl.multiple_of(head * DV, DV), DV)].T

    @pl.when(head == 0)
    def _():
        cb = dot_f32(obasis_t[...], cot_ref[...], ((1,), (1,)))
        high, low = split_two(cb)
        cb_high[...] = high
        cb_low[...] = low
        high, low = split_two(dot_f32(vbasis_t[...], input_ref[...], ((1,), (1,))))
        vcot = vcot_ref[...]
        vproj_ref[...] += dot_f32(high, vcot) + dot_f32(low, vcot)

    columns = pl.ds(pl.multiple_of(head * DV, DV), DV)
    lam = lam_ref[head]
    lane = lax.broadcasted_iota(jnp.int32, (span, DV), 1)
    query = query_ref[:, columns].astype(F32) * DH ** (-0.5)
    query_one = jnp.where(lane < DH, query, 0.0).astype(BF16)
    query_two = jnp.where(lane < DH, 0.0, query).astype(BF16)

    def attend(width, open_from):
        def tiles():
            return range(0, width, TILE)

        peak_one = jnp.full((8, span), -jnp.inf, F32)
        peak_two = peak_one
        for at in tiles():
            keys = key_ref[at : at + TILE, columns]
            one = dot_f32(keys, query_one, ((1,), (1,)))
            two = dot_f32(keys, query_two, ((1,), (1,)))
            if at >= open_from:
                key_pos = at + lax.broadcasted_iota(jnp.int32, (TILE, span), 0)
                query_pos = block * span + lax.broadcasted_iota(jnp.int32, (TILE, span), 1)
                causal = key_pos <= query_pos
                one = jnp.where(causal, one, -jnp.inf)
                two = jnp.where(causal, two, -jnp.inf)
            score_one[at : at + TILE, :] = one
            score_two[at : at + TILE, :] = two
            peak_one = jnp.maximum(peak_one, fold_rows(one, jnp.max))
            peak_two = jnp.maximum(peak_two, fold_rows(two, jnp.max))
        peak_one = jnp.max(peak_one, axis=0, keepdims=True)
        peak_two = jnp.max(peak_two, axis=0, keepdims=True)
        sum_one = jnp.zeros((8, span), F32)
        sum_two = sum_one
        for at in tiles():
            one = jnp.exp(score_one[at : at + TILE, :] - peak_one)
            two = jnp.exp(score_two[at : at + TILE, :] - peak_two)
            score_one[at : at + TILE, :] = one
            score_two[at : at + TILE, :] = two
            sum_one += fold_rows(one, jnp.sum)
            sum_two += fold_rows(two, jnp.sum)
        rate_one = 1.0 / jnp.sum(sum_one, axis=0, keepdims=True)
        rate_two = lam / jnp.sum(sum_two, axis=0, keepdims=True)
        for at in tiles():
            mix_ref[at : at + TILE, :] = (
                score_one[at : at + TILE, :] * rate_one - score_two[at : at + TILE, :] * rate_two
            ).astype(BF16)
        raw = dot_f32(value_t[head, :, :width], mix_ref[:width, :])
        mean_sq = jnp.mean(raw * raw, axis=0, keepdims=True)
        out_t = (raw * lax.rsqrt(mean_sq + EPSILON_NORM) * gain_ref[...]).astype(BF16)
        oproj_ref[:, columns] += dot_f32(cb_high[...], out_t, ((1,), (1,))) + dot_f32(
            cb_low[...], out_t, ((1,), (1,))
        )

    step = min(2 * span, seq_len)
    for width in range(step, seq_len + 1, step):
        lowest = (width - step) // span

        @pl.when((block >= lowest) & (block < width // span))
        def _(width=width):
            attend(width, width - step)


def local_grads(
    query_rows, key_rows, value_rows, mix_lambda, head_gain, out_cotangent, layer_input,
    value_cotangent, out_basis, value_basis,
):
    seq_len, cols = query_rows.shape
    heads = mix_lambda.shape[0]
    width = out_cotangent.shape[1]
    rank = out_basis.shape[1]
    span = min(TILE, seq_len)
    blocks = seq_len // span
    rows_spec = lambda wide: pl.BlockSpec((span, wide), lambda i, h: (i, 0))
    whole = lambda a, b: pl.BlockSpec((a, b), lambda i, h: (0, 0))
    return pl.pallas_call(
        grads_kernel,
        grid=(blocks, heads),
        out_shape=(
            jax.ShapeDtypeStruct((rank, cols), F32),
            jax.ShapeDtypeStruct((rank, cols), F32),
        ),
        in_specs=[
            pl.BlockSpec(memory_space=pltpu.SMEM),
            rows_spec(cols),
            whole(seq_len, cols),
            whole(seq_len, cols),
            whole(DV, 1),
            rows_spec(width),
            rows_spec(width),
            rows_spec(cols),
            whole(width, rank),
            whole(width, rank),
        ],
        out_specs=(whole(rank, cols), whole(rank, cols)),
        scratch_shapes=[
            pltpu.VMEM((seq_len, span), F32),
            pltpu.VMEM((seq_len, span), F32),
            pltpu.VMEM((seq_len, span), BF16),
            pltpu.VMEM((heads, DV, seq_len), BF16),
            pltpu.VMEM((rank, width), BF16),
            pltpu.VMEM((rank, width), BF16),
            pltpu.VMEM((rank, span), BF16),
            pltpu.VMEM((rank, span), BF16),
        ],
        compiler_params=pltpu.CompilerParams(
            dimension_semantics=("arbitrary", "arbitrary"),
            vmem_limit_bytes=60 * 1024 * 1024,
        ),
        name="grads",
    )(
        mix_lambda, query_rows, key_rows, value_rows, head_gain.reshape(DV, 1),
        out_cotangent, layer_input, value_cotangent, out_basis, value_basis,
    )


def moment_step(proj, first, second):
    new_first = BETA_ONE * first + (1.0 - BETA_ONE) * proj
    new_second = BETA_TWO * second + (1.0 - BETA_TWO) * proj * proj
    direction = new_first / (jnp.sqrt(new_second) + EPSILON_ADAM)
    return (new_first, new_second, direction)


def finish_kernel(
    fs_count, tp_count,
    opart, vpart, ofirst, osecond, vfirst, vsecond, obasis, vbasis, oweight, vweight,
    ostep, vstep, onew, vnew, ocopy, vcopy, ofirst_new, osecond_new, vfirst_new, vsecond_new,
    got, dirs, squares, squares_got,
    scatter_send, scatter_recv, ring_send, ring_recv, copy_send, copy_recv, sq_send, sq_recv,
):
    me = lax.axis_index("fs")
    my_tp = lax.axis_index("tp")
    half_count = fs_count // 2
    rank_share = ofirst.shape[0]
    cols = ofirst.shape[1]
    row_share = vweight.shape[0]
    mesh_ids = pl.DeviceIdType.MESH

    place = jnp.where(me % 2 == 0, me // 2, fs_count - 1 - me // 2)

    def owner(at):
        at = lax.rem(at + 2 * fs_count, fs_count)
        return jnp.where(at < half_count, 2 * at, 2 * (fs_count - 1 - at) + 1)

    def fs_peer(gap):
        return lax.rem(me + gap, fs_count)

    def tp_peer(gap):
        return lax.rem(my_tp + gap, tp_count)

    barrier = pltpu.get_barrier_semaphore()
    for gap in range(1, fs_count):
        pl.semaphore_signal(
            barrier, inc=1, device_id=(fs_peer(gap), my_tp), device_id_type=mesh_ids
        )
    for gap in range(1, tp_count):
        pl.semaphore_signal(
            barrier, inc=1, device_id=(me, tp_peer(gap)), device_id_type=mesh_ids
        )
    pl.semaphore_wait(barrier, fs_count + tp_count - 2)

    def share(index, size):
        return pl.ds(pl.multiple_of(index * size, size), size)

    parts = (vpart, opart)
    scatters = ([], [])
    for mat in range(2):
        for gap in range(1, fs_count):
            peer = fs_peer(gap)
            copy = pltpu.make_async_remote_copy(
                src_ref=parts[mat].at[share(peer, rank_share)],
                dst_ref=got.at[mat, gap - 1],
                send_sem=scatter_send.at[mat, gap - 1],
                recv_sem=scatter_recv.at[mat, gap - 1],
                device_id=(peer, my_tp),
                device_id_type=mesh_ids,
            )
            copy.start()
            scatters[mat].append(copy)

    def ring(blocks, sems_send, sems_recv):
        def make(mat, step, way):
            origin = owner(place - step if way == 0 else place + step)
            split = way if step == half_count - 1 else None
            ref = blocks[mat](origin, split)
            target = owner(place + 1 if way == 0 else place - 1)
            return pltpu.make_async_remote_copy(
                src_ref=ref,
                dst_ref=ref,
                send_sem=sems_send.at[mat, way, step],
                recv_sem=sems_recv.at[mat, way, step],
                device_id=(target, my_tp),
                device_id_type=mesh_ids,
            )

        def arrival(mat, step, way):
            origin = owner(place - 1 - step if way == 0 else place + 1 + step)
            split = way if step == half_count - 1 else None
            ref = blocks[mat](origin, split)
            return pltpu.make_async_remote_copy(
                src_ref=ref,
                dst_ref=ref,
                send_sem=sems_send.at[mat, way, step],
                recv_sem=sems_recv.at[mat, way, step],
                device_id=(owner(place + 1), my_tp),
                device_id_type=mesh_ids,
            )

        started = []

        def begin(mat):
            for way in range(2):
                copy = make(mat, 0, way)
                copy.start()
                started.append(copy)

        def drain():
            for step in range(half_count):
                for mat in range(len(blocks)):
                    for way in range(2):
                        arrival(mat, step, way).wait_recv()
                        if step + 1 < half_count:
                            copy = make(mat, step + 1, way)
                            copy.start()
                            started.append(copy)
            for copy in started:
                copy.wait_send()

        return begin, drain

    def halved(start, size, split):
        if split is None:
            return pl.ds(pl.multiple_of(start, size), size)
        return pl.ds(pl.multiple_of(start + split * (size // 2), size // 2), size // 2)

    begin, drain = ring(
        [
            lambda at, split, mat=mat: dirs.at[mat, halved(at * rank_share, rank_share, split)]
            for mat in range(2)
        ],
        ring_send, ring_recv,
    )
    moments = (
        (vfirst, vsecond, vfirst_new, vsecond_new),
        (ofirst, osecond, ofirst_new, osecond_new),
    )
    for mat in range(2):
        proj = parts[mat][share(me, rank_share), :]
        for gap in range(1, fs_count):
            scatters[mat][gap - 1].wait_recv()
            proj += got[mat, gap - 1]
        first, second, first_new, second_new = moments[mat]
        new_first, new_second, direction = moment_step(proj, first[...], second[...])
        dirs[mat, share(me, rank_share), :] = direction
        begin(mat)
        first_new[...] = new_first
        second_new[...] = new_second
    drain()

    for mat in range(2):
        whole = dirs[mat]
        squared = fold_rows(whole * whole, jnp.sum)
        total = squared[:, :128]
        for at in range(128, cols, 128):
            total += squared[:, at : at + 128]
        squares[mat] = total
    exchanges = []
    for gap in range(1, tp_count):
        copy = pltpu.make_async_remote_copy(
            src_ref=squares,
            dst_ref=squares_got.at[gap - 1],
            send_sem=sq_send.at[gap - 1],
            recv_sem=sq_recv.at[gap - 1],
            device_id=(me, tp_peer(gap)),
            device_id_type=mesh_ids,
        )
        copy.start()
        exchanges.append(copy)

    high, low = split_two(dirs[0])
    vstep[...] = dot_f32(vbasis[...], high) + dot_f32(vbasis[...], low)
    high, low = split_two(dirs[1])
    ostep[...] = dot_f32(high, obasis[...], ((0,), (1,))) + dot_f32(
        low, obasis[...], ((0,), (1,))
    )
    for copy in exchanges:
        copy.wait_recv()
    entry_count = rank_share * fs_count * cols * tp_count

    def clip_of(mat):
        total = squares[mat]
        for gap in range(1, tp_count):
            total += squares_got[gap - 1, mat]
        total = jnp.sum(jnp.sum(total, axis=0, keepdims=True), axis=1, keepdims=True)
        return jnp.minimum(1.0, CLIP_RMS * math.sqrt(entry_count) / jnp.sqrt(total))

    begin, drain = ring(
        [
            lambda at, split: vcopy.at[halved(at * row_share, row_share, split)],
            lambda at, split: ocopy.at[
                slice(None) if split is None else pl.ds(split * (cols // 2), cols // 2),
                share(at, row_share),
            ],
        ],
        copy_send, copy_recv,
    )
    step = clip_of(0) * vstep[...]
    vstep[...] = step
    weight = vweight[...] - LEARN_RATE * step
    vnew[...] = weight
    vcopy[share(me, row_share), :] = weight.astype(BF16)
    begin(0)
    step = clip_of(1) * ostep[...]
    ostep[...] = step
    weight = oweight[...] - LEARN_RATE * step
    onew[...] = weight
    ocopy[:, share(me, row_share)] = weight.astype(BF16)
    begin(1)
    drain()
    for copy in scatters[0] + scatters[1] + exchanges:
        copy.wait_send()


def finish(
    out_part, value_part, out_first, out_second, value_first, value_second, out_rows_b,
    value_rows_b, out_weight, value_weight,
):
    fs_count = lax.axis_size("fs")
    tp_count = lax.axis_size("tp")
    rank, cols = out_part.shape
    row_share = value_weight.shape[0]
    like = lambda a: jax.ShapeDtypeStruct(a.shape, a.dtype)
    half_count = fs_count // 2
    dma = pltpu.SemaphoreType.DMA
    return pl.pallas_call(
        functools.partial(finish_kernel, fs_count, tp_count),
        out_shape=(
            like(out_weight), like(value_weight), like(out_weight), like(value_weight),
            jax.ShapeDtypeStruct((cols, row_share * fs_count), BF16),
            jax.ShapeDtypeStruct((row_share * fs_count, cols), BF16),
            like(out_first), like(out_second), like(value_first), like(value_second),
        ),
        in_specs=[pl.BlockSpec(memory_space=pltpu.VMEM)] * 10,
        out_specs=tuple([pl.BlockSpec(memory_space=pltpu.VMEM)] * 10),
        scratch_shapes=[
            pltpu.VMEM((2, fs_count - 1, rank // fs_count, cols), F32),
            pltpu.VMEM((2, rank, cols), F32),
            pltpu.VMEM((2, 8, 128), F32),
            pltpu.VMEM((tp_count - 1, 2, 8, 128), F32),
            dma((2, fs_count - 1)), dma((2, fs_count - 1)),
            dma((2, 2, half_count)), dma((2, 2, half_count)),
            dma((2, 2, half_count)), dma((2, 2, half_count)),
            dma((tp_count - 1,)), dma((tp_count - 1,)),
        ],
        compiler_params=pltpu.CompilerParams(
            collective_id=0, has_side_effects=True, vmem_limit_bytes=48 * 1024 * 1024
        ),
        name="finish",
    )(
        out_part, value_part, out_first, out_second, value_first, value_second, out_rows_b,
        value_rows_b, out_weight, value_weight,
    )


def body(
    query_rows, key_rows, value_rows, mix_lambda, head_gain, out_cotangent, layer_input,
    value_cotangent, out_weight, value_weight, out_basis, value_basis, out_first, out_second,
    value_first, value_second,
):
    row_share = out_cotangent.shape[1] // lax.axis_size("fs")
    row_base = lax.axis_index("fs") * row_share
    out_rows_b = lax.dynamic_slice_in_dim(out_basis, row_base, row_share, 0)
    value_rows_b = lax.dynamic_slice_in_dim(value_basis, row_base, row_share, 0)
    out_part, value_part = local_grads(
        query_rows, key_rows, value_rows, mix_lambda, head_gain, out_cotangent, layer_input,
        value_cotangent, out_basis, value_basis,
    )
    return finish(
        out_part, value_part, out_first, out_second, value_first, value_second, out_rows_b,
        value_rows_b, out_weight, value_weight,
    )


def solution(mesh):
    placed = (
        P("fs", "tp"),
        P("fs", "tp"),
        P("fs", "tp"),
        P("tp"),
        P(),
        P("fs", None),
        P("fs", None),
        P("fs", "tp"),
        P("tp", "fs"),
        P("fs", "tp"),
        P(),
        P(),
        P("fs", "tp"),
        P("fs", "tp"),
        P("fs", "tp"),
        P("fs", "tp"),
    )
    return jax.shard_map(
        body,
        mesh=mesh,
        in_specs=placed,
        out_specs=(
            P("tp", "fs"),
            P("fs", "tp"),
            P("tp", "fs"),
            P("fs", "tp"),
            P("tp", None),
            P(None, "tp"),
            P("fs", "tp"),
            P("fs", "tp"),
            P("fs", "tp"),
            P("fs", "tp"),
        ),
        check_vma=False,
    )
```

profile of v0, /device:TPU:0, one launch (start us, length us, event | category | flops | bytes accessed | tf_op | source)
XLA Modules:
  0.0 181.6 jit_solution(16358269975436792741)
XLA Ops:
  0.6 1.4 copy.26.gain_ref
  2.0 1.0 constant_dynamic-slice_fusion
  3.0 0.0 copy-start
  3.0 0.0 copy-start.1
  3.0 0.0 copy-start.4
  3.1 0.0 copy-start.5
  3.1 0.0 copy-start.6
  3.1 0.0 copy-start.7
  3.1 75.3 %grads.1 = (f32[256,512]{1,0:T(8,128)}, f32[256,512]{1,0:T(8,128)}) custom-call(f32[4]{0:T(128)} %lam_ref.1, bf16[2048,512]{1,0:T(8,128)(2,1)} %query_ref.1, bf16[2048,512]{1,0:T(8,128)(2,1)} %key_ref.1, bf16[2048,512]{1,0:T(8,128)(2,1)} %value_ref.1, f32[128,1]{1,0:T(8,128)} %copy.26.gain_ref, bf16[2048,2048]{1,0:T(8,128)(2,1)} %cot_ref.1, ...), custom_call_target="tpu_custom_call" | custom-call | tf_op jit(solution)/shard_map/grads/pallas_call | solution.py:143
  78.4 0.0 copy-done
  78.4 0.0 copy-done.1
  78.4 0.0 copy-done.4
  78.5 0.0 copy-done.5
  78.5 0.0 copy-done.6
  78.5 0.0 copy-done.7
  78.5 0.0 copy-start.2
  78.5 1.0 copy-done.2
  79.5 0.0 copy-start.3
  79.5 1.0 copy-done.3
  80.6 91.7 %finish.1 = (f32[512,256]{1,0:T(8,128)S(1)}, f32[256,512]{1,0:T(8,128)S(1)}, f32[512,256]{1,0:T(8,128)S(1)}, f32[256,512]{1,0:T(8,128)S(1)}, bf16[512,2048]{1,0:...) custom-call(f32[256,512]{1,0:T(8,128)S(1)} %copy-done.2, ...), custom_call_target="tpu_custom_call" | custom-call | tf_op jit(solution)/shard_map/finish/pallas_call | solution.py:402
  172.3 0.0 copy-start.9
  172.3 0.8 copy.37
  173.1 0.8 copy.38
  173.9 0.8 copy.39
  174.6 0.8 copy.40
  175.4 0.0 copy-done.9
  175.4 0.0 copy-start.8
  175.4 1.3 copy.41
  176.8 1.0 copy-done.8
  177.8 1.3 copy.42
  179.1 0.6 copy.43
  179.7 0.6 copy.44
  180.4 0.6 copy.45
  181.0 0.6 copy.46
Async XLA Ops:
  3.0 75.4 %copy-start = (f32[512,256]{1,0:T(8,128)S(1)}, f32[512,256]{1,0:T(8,128)}, u32[]{:S(2)}) copy-start(f32[512,256]{1,0:T(8,128)} %oweight.1) | copy-start | bytes 1572868
  3.0 75.4 %copy-start.1 = (f32[256,512]{1,0:T(8,128)S(1)}, f32[256,512]{1,0:T(8,128)}, u32[]{:S(2)}) copy-start(f32[256,512]{1,0:T(8,128)} %vweight.1) | copy-start | bytes 1572868
  3.0 75.4 %copy-start.4 = (f32[32,512]{1,0:T(8,128)S(1)}, f32[32,512]{1,0:T(8,128)}, u32[]{:S(2)}) copy-start(f32[32,512]{1,0:T(8,128)} %ofirst.1) | copy-start | bytes 196612
  3.1 75.4 %copy-start.5 = (f32[32,512]{1,0:T(8,128)S(1)}, f32[32,512]{1,0:T(8,128)}, u32[]{:S(2)}) copy-start(f32[32,512]{1,0:T(8,128)} %osecond.1) | copy-start | bytes 196612
  3.1 75.4 %copy-start.6 = (f32[32,512]{1,0:T(8,128)S(1)}, f32[32,512]{1,0:T(8,128)}, u32[]{:S(2)}) copy-start(f32[32,512]{1,0:T(8,128)} %vfirst.1) | copy-start | bytes 196612
  3.1 75.4 %copy-start.7 = (f32[32,512]{1,0:T(8,128)S(1)}, f32[32,512]{1,0:T(8,128)}, u32[]{:S(2)}) copy-start(f32[32,512]{1,0:T(8,128)} %vsecond.1) | copy-start | bytes 196612
  78.5 1.0 copy-start.2
  79.5 1.0 copy-start.3
  172.3 3.2 %copy-start.9 = (bf16[512,2048]{1,0:T(8,128)(2,1)S(1)}, bf16[512,2048]{1,0:T(8,128)(2,1)}, u32[]{:S(2)}) copy-start(bf16[512,2048]{1,0:T(8,128)(2,1)} %get-tuple-element.30) | copy-start | bytes 6291460
  175.4 2.3 %copy-start.8 = (bf16[2048,512]{1,0:T(8,128)(2,1)S(1)}, bf16[2048,512]{1,0:T(8,128)(2,1)}, u32[]{:S(2)}) copy-start(bf16[2048,512]{1,0:T(8,128)(2,1)} %get-tuple-element.31) | copy-start | bytes 6291460
where the time goes:
time: 182 us
  Pallas kernels  167 us (92%)
  local copies, waits for them, and re-layouts  13.9 us (8%)
    pallas_call x1, Pallas kernels, finish(): pl.pallas_call(functools.partial(finish_kernel, fs_count, tp_count), out_...  91.7 us
    pallas_call x1, Pallas kernels, local_grads(): pl.pallas_call(grads_kernel, grid=(blocks, heads), out_shape=(jax.ShapeDt...  75.3 us
    unnamed x30, local copies, waits for them, and re-layouts  11.5 us

commit v1 on v0

v1 whole, which is shorter than its diff:
```python
import functools
import math

import jax
import jax.numpy as jnp
from jax import lax
from jax.experimental import pallas as pl
from jax.experimental.pallas import tpu as pltpu
from jax.sharding import PartitionSpec as P

DH = 64
DV = 128


EPSILON_NORM = 1e-05
EPSILON_ADAM = 1e-08
BETA_ONE = 0.9
BETA_TWO = 0.95
CLIP_RMS = 1.0
LEARN_RATE = 0.01
TILE = 256
SLOTS = 4
PAIR = 2
LOG2E = 1.4426950408889634
F32 = jnp.float32
BF16 = jnp.bfloat16


def dot_f32(left, right, dims=((1,), (0,))):
    return lax.dot_general(left, right, (dims, ((), ())), preferred_element_type=F32)


def split_two(wide):
    high = wide.astype(BF16)
    return high, (wide - high.astype(F32)).astype(BF16)


def fold_rows(tile, op):
    rows, cols = tile.shape
    return op(tile.reshape(rows // 8, 8, cols), axis=0)


def moment_step(proj, first, second):
    new_first = BETA_ONE * first + (1.0 - BETA_ONE) * proj
    new_second = BETA_TWO * second + (1.0 - BETA_TWO) * proj * proj
    direction = new_first / (jnp.sqrt(new_second) + EPSILON_ADAM)
    return (new_first, new_second, direction)


def step_kernel(
    fs_count, tp_count,
    lam_ref, gain_ref, query_h, key_h, value_h, cot_h, input_h, vcot_h, obasis_h, vbasis_h,
    oweight_h, vweight_h, ofirst_h, osecond_h, vfirst_h, vsecond_h,
    ostep, vstep, onew, vnew, ocopy, vcopy, ofirst_new, osecond_new, vfirst_new, vsecond_new,
    query_v, key_v, value_v, vcot_v, obasis_v, vbasis_v, oweight, vweight,
    ofirst, osecond, vfirst, vsecond, chunks,
    score_one, score_two, mix_ref, value_t, obasis_t, vbasis_t, cb_high, cb_low, gain_t, tri,
    vproj, oproj, vgot, ogot, vdirs, odirs, squares, squares_got,
    load_sem, chunk_sem, vs_send, vs_recv, os_send, os_recv, vg_send, vg_recv, og_send, og_recv,
    sq_send, sq_recv, ring_send, ring_recv,
):
    me = lax.axis_index("fs")
    my_tp = lax.axis_index("tp")
    half_count = fs_count // 2
    rank_share, cols = ofirst.shape
    row_share = vweight.shape[0]
    seq_len = query_v.shape[0]
    blocks = seq_len // TILE
    pairs = oproj.shape[0]
    wide = PAIR * DV
    mesh_ids = pl.DeviceIdType.MESH

    def fs_peer(gap):
        return lax.rem(me + gap, fs_count)

    def tp_peer(gap):
        return lax.rem(my_tp + gap, tp_count)

    def share(index, size):
        return pl.ds(pl.multiple_of(index * size, size), size)

    barrier = pltpu.get_barrier_semaphore()
    for gap in range(1, fs_count):
        pl.semaphore_signal(
            barrier, inc=1, device_id=(fs_peer(gap), my_tp), device_id_type=mesh_ids
        )
    for gap in range(1, tp_count):
        pl.semaphore_signal(
            barrier, inc=1, device_id=(me, tp_peer(gap)), device_id_type=mesh_ids
        )

    def chunk_copy(source, at, slot):
        return pltpu.make_async_copy(
            source.at[share(at, TILE)], chunks.at[slot], chunk_sem.at[slot]
        )

    def load(index, source, target):
        copy = pltpu.make_async_copy(source, target, load_sem.at[index])
        copy.start()
        return copy

    early = [load(0, vbasis_h, vbasis_v)]
    for at in range(SLOTS - 1):
        chunk_copy(input_h, at, at).start()
    early.append(load(1, vcot_h, vcot_v))
    chunk_copy(input_h, SLOTS - 1, SLOTS - 1).start()
    early.append(load(2, obasis_h, obasis_v))
    attention = [
        load(3, query_h, query_v), load(4, key_h, key_v), load(5, value_h, value_v),
    ]
    late = [
        load(6, vfirst_h, vfirst), load(7, vsecond_h, vsecond), load(8, ofirst_h, ofirst),
        load(9, osecond_h, osecond), load(10, vweight_h, vweight), load(11, oweight_h, oweight),
    ]

    key_pos = lax.broadcasted_iota(jnp.int32, (TILE, TILE), 0)
    query_pos = lax.broadcasted_iota(jnp.int32, (TILE, TILE), 1)
    tri[...] = jnp.where(key_pos <= query_pos, 0.0, -jnp.inf)
    gain_t[...] = jnp.broadcast_to(gain_ref[...], (DV, DV)).T
    vproj[...] = jnp.zeros_like(vproj)
    oproj[...] = jnp.zeros_like(oproj)

    early[0].wait()
    vbasis_t[...] = vbasis_v[...].T
    early[1].wait()

    def value_block(at, carry):
        slot = lax.rem(at, SLOTS)
        chunk_copy(input_h, at, slot).wait()
        high, low = split_two(dot_f32(vbasis_t[...], chunks[slot], ((1,), (1,))))
        vcot = vcot_v[share(at, TILE), :]
        vproj[...] += dot_f32(high, vcot) + dot_f32(low, vcot)

        @pl.when(at < blocks - SLOTS)
        def _():
            chunk_copy(input_h, at + SLOTS, slot).start()

        @pl.when(at >= blocks - SLOTS)
        def _():
            chunk_copy(cot_h, at - (blocks - SLOTS), slot).start()

        return carry

    lax.fori_loop(0, blocks, value_block, 0)
    pl.semaphore_wait(barrier, fs_count + tp_count - 2)

    def exchange(source, target, send, recv):
        copies = []
        for gap in range(1, fs_count):
            peer = fs_peer(gap)
            copies.append(
                pltpu.make_async_remote_copy(
                    src_ref=source(peer),
                    dst_ref=target(gap),
                    send_sem=send.at[gap - 1],
                    recv_sem=recv.at[gap - 1],
                    device_id=(peer, my_tp),
                    device_id_type=mesh_ids,
                )
            )
        return copies

    vscatter = exchange(
        lambda peer: vproj.at[share(peer, rank_share)], lambda gap: vgot.at[gap - 1],
        vs_send, vs_recv,
    )
    vgather = exchange(
        lambda peer: vdirs.at[share(me, rank_share)],
        lambda gap: vdirs.at[share(me, rank_share)], vg_send, vg_recv,
    )
    oscatter = [
        exchange(
            lambda peer, at=at: oproj.at[at, share(peer, rank_share)],
            lambda gap, at=at: ogot.at[at, gap - 1], os_send.at[at], os_recv.at[at],
        )
        for at in range(pairs)
    ]
    ogather = [
        exchange(
            lambda peer, at=at: odirs.at[at, share(me, rank_share)],
            lambda gap, at=at: odirs.at[at, share(me, rank_share)],
            og_send.at[at], og_recv.at[at],
        )
        for at in range(pairs)
    ]

    def start_all(copies):
        for copy in copies:
            copy.start()

    def square_copies(mat):
        return [
            pltpu.make_async_remote_copy(
                src_ref=squares.at[mat],
                dst_ref=squares_got.at[mat, gap - 1],
                send_sem=sq_send.at[mat, gap - 1],
                recv_sem=sq_recv.at[mat, gap - 1],
                device_id=(me, tp_peer(gap)),
                device_id_type=mesh_ids,
            )
            for gap in range(1, tp_count)
        ]

    def put_squares(mat, tiles):
        total = jnp.zeros((8, 128), F32)
        for tile in tiles:
            squared = fold_rows(tile * tile, jnp.sum)
            for at in range(0, squared.shape[1], 128):
                total += squared[:, at : at + 128]
        squares[mat] = total
        start_all(square_copies(mat))

    entry_count = rank_share * fs_count * cols * tp_count

    def clip_of(mat):
        total = squares[mat]
        copies = square_copies(mat)
        for gap in range(1, tp_count):
            copies[gap - 1].wait_recv()
            total += squares_got[mat, gap - 1]
        total = jnp.sum(jnp.sum(total, axis=0, keepdims=True), axis=1, keepdims=True)
        return jnp.minimum(1.0, CLIP_RMS * math.sqrt(entry_count) / jnp.sqrt(total))

    place = jnp.where(me % 2 == 0, me // 2, fs_count - 1 - me // 2)

    def owner(at):
        at = lax.rem(at + 2 * fs_count, fs_count)
        return jnp.where(at < half_count, 2 * at, 2 * (fs_count - 1 - at) + 1)

    def halved(start, size, split):
        if split is None:
            return pl.ds(pl.multiple_of(start, size), size)
        return pl.ds(pl.multiple_of(start + split * (size // 2), size // 2), size // 2)

    def ring_block(mat, at, split):
        if mat == 0:
            return vcopy.at[halved(at * row_share, row_share, split)]
        rows = slice(None) if split is None else pl.ds(split * (cols // 2), cols // 2)
        return ocopy.at[rows, share(at, row_share)]

    def ring_copy(mat, step, way, arriving):
        back = step + 1 if arriving else step
        origin = owner(place - back if way == 0 else place + back)
        ref = ring_block(mat, origin, way if step == half_count - 1 else None)
        return pltpu.make_async_remote_copy(
            src_ref=ref,
            dst_ref=ref,
            send_sem=ring_send.at[mat, way, step],
            recv_sem=ring_recv.at[mat, way, step],
            device_id=(owner(place + 1 if way == 0 else place - 1), my_tp),
            device_id_type=mesh_ids,
        )

    def ring_begin(mat):
        for way in range(2):
            ring_copy(mat, 0, way, False).start()

    def ring_forward(mat, step):
        for way in range(2):
            ring_copy(mat, step, way, True).wait_recv()
            if step + 1 < half_count:
                ring_copy(mat, step + 1, way, False).start()

    def value_moments():
        for copy in late:
            copy.wait()
        proj = vproj[share(me, rank_share), :]
        for gap in range(1, fs_count):
            vscatter[gap - 1].wait_recv()
            proj += vgot[gap - 1]
        new_first, new_second, direction = moment_step(proj, vfirst[...], vsecond[...])
        vdirs[share(me, rank_share), :] = direction
        start_all(vgather)
        vfirst_new[...] = new_first
        vsecond_new[...] = new_second

    def value_squares():
        for copy in vgather:
            copy.wait_recv()
        put_squares(0, [vdirs[...]])
        high, low = split_two(vdirs[...])
        rows = vbasis_v[share(me, row_share), :]
        vstep[...] = dot_f32(rows, high) + dot_f32(rows, low)

    def value_update():
        step = clip_of(0) * vstep[...]
        vstep[...] = step
        weight = vweight[...] - LEARN_RATE * step
        vnew[...] = weight
        vcopy[share(me, row_share), :] = weight.astype(BF16)
        ring_begin(0)

    def out_moments(at):
        span = slice(at * wide, (at + 1) * wide)
        proj = oproj[at, share(me, rank_share), :]
        for gap in range(1, fs_count):
            oscatter[at][gap - 1].wait_recv()
            proj += ogot[at, gap - 1]
        new_first, new_second, direction = moment_step(proj, ofirst[:, span], osecond[:, span])
        odirs[at, share(me, rank_share), :] = direction
        start_all(ogather[at])
        ofirst_new[:, span] = new_first
        osecond_new[:, span] = new_second

    def out_arrived(at):
        for copy in ogather[at]:
            copy.wait_recv()

    def out_step(at):
        rows = obasis_v[share(me, row_share), :]
        high, low = split_two(odirs[at])
        ostep[at * wide : (at + 1) * wide, :] = dot_f32(high, rows, ((0,), (1,))) + dot_f32(
            low, rows, ((0,), (1,))
        )

    def out_update():
        put_squares(1, [odirs[at] for at in range(pairs)])
        out_step(pairs - 1)
        step = clip_of(1) * ostep[...]
        ostep[...] = step
        weight = oweight[...] - LEARN_RATE * step
        onew[...] = weight
        ocopy[:, share(me, row_share)] = weight.astype(BF16)
        ring_begin(1)

    start_all(vscatter)

    early[2].wait()
    obasis_t[...] = obasis_v[...].T

    def cot_block(at, carry):
        slot = lax.rem(at, SLOTS)
        chunk_copy(cot_h, at, slot).wait()
        high, low = split_two(dot_f32(obasis_t[...], chunks[slot], ((1,), (1,))))
        cb_high[at] = high
        cb_low[at] = low

        @pl.when(at < blocks - SLOTS)
        def _():
            chunk_copy(cot_h, at + SLOTS, slot).start()

        return carry

    lax.fori_loop(0, blocks, cot_block, 0)
    for copy in attention:
        copy.wait()
    for head in range(pairs * PAIR):
        value_t[head] = value_v[:, head * DV : (head + 1) * DV].T

    lane = lax.broadcasted_iota(jnp.int32, (TILE, DV), 1)

    def attend(block, pair, which):
        head = pair * PAIR + which
        columns = pl.ds(pl.multiple_of(head * DV, DV), DV)
        lam = lam_ref[head]
        width = (block + 1) * TILE
        query = query_v[block * TILE : (block + 1) * TILE, columns].astype(F32)
        query = query * (DH ** (-0.5) * LOG2E)
        parts_one = split_two(jnp.where(lane < DH, query, 0.0))
        parts_two = split_two(jnp.where(lane < DH, 0.0, query))
        query_one = jnp.concatenate(parts_one, axis=1)
        query_two = jnp.concatenate(parts_two, axis=1)
        peak_one = jnp.full((8, TILE), -jnp.inf, F32)
        peak_two = peak_one
        for at in range(0, width, TILE):
            keys = key_v[at : at + TILE, columns]
            keys = jnp.concatenate([keys, keys], axis=1)
            one = dot_f32(keys, query_one, ((1,), (1,)))
            two = dot_f32(keys, query_two, ((1,), (1,)))
            if at == width - TILE:
                one = one + tri[...]
                two = two + tri[...]
            score_one[at : at + TILE, :] = one
            score_two[at : at + TILE, :] = two
            peak_one = jnp.maximum(peak_one, fold_rows(one, jnp.max))
            peak_two = jnp.maximum(peak_two, fold_rows(two, jnp.max))
        peak_one = jnp.max(peak_one, axis=0, keepdims=True)
        peak_two = jnp.max(peak_two, axis=0, keepdims=True)
        sum_one = jnp.zeros((8, TILE), F32)
        sum_two = sum_one
        for at in range(0, width, TILE):
            one = jnp.exp2(score_one[at : at + TILE, :] - peak_one)
            two = jnp.exp2(score_two[at : at + TILE, :] - peak_two)
            score_one[at : at + TILE, :] = one
            score_two[at : at + TILE, :] = two
            sum_one += fold_rows(one, jnp.sum)
            sum_two += fold_rows(two, jnp.sum)
        rate_one = 1.0 / jnp.sum(sum_one, axis=0, keepdims=True)
        rate_two = lam / jnp.sum(sum_two, axis=0, keepdims=True)
        for at in range(0, width, TILE):
            mix_ref[at : at + TILE, :] = (
                score_one[at : at + TILE, :] * rate_one - score_two[at : at + TILE, :] * rate_two
            ).astype(BF16)
        raw = dot_f32(value_t[head, :, :width], mix_ref[:width, :])
        mean_sq = jnp.mean(raw * raw, axis=0, keepdims=True)
        gain = jnp.concatenate([gain_t[...]] * (TILE // DV), axis=1)
        out_t = (raw * lax.rsqrt(mean_sq + EPSILON_NORM) * gain).astype(BF16)
        span = slice(which * DV, (which + 1) * DV)
        oproj[pair, :, span] += dot_f32(cb_high[block], out_t, ((1,), (1,))) + dot_f32(
            cb_low[block], out_t, ((1,), (1,))
        )

    events = {}

    def plan(pair, item, action):
        events.setdefault((pair, item), []).append(action)

    last = 2 * blocks
    at = (8, 13, 14, 17, 21, 24, 27)
    actions = [value_moments, value_squares, value_update] + [
        functools.partial(ring_forward, 0, step) for step in range(half_count)
    ]
    for tick, action in zip(at, actions):
        plan(tick // last, tick % last, action)
    for pair in range(pairs - 1):
        plan(pair + 1, 2, functools.partial(start_all, oscatter[pair]))
        plan(pair + 1, 10, functools.partial(out_moments, pair))
        plan(pair + 1, 14, functools.partial(out_arrived, pair))
        plan(pair + 1, 14, functools.partial(out_step, pair))

    def pair_items(pair, carry):
        for item in range(last):
            for when in range(pairs):
                for action in events.get((when, item), []):
                    pl.when(pair == when)(action)
            attend(item // PAIR, pair, item % PAIR)
        return carry

    lax.fori_loop(0, pairs, pair_items, 0)
    start_all(oscatter[pairs - 1])
    for (pair, item) in sorted(events):
        if pair >= pairs:
            for action in events[(pair, item)]:
                action()
    out_moments(pairs - 1)
    out_arrived(pairs - 1)
    out_update()
    for step in range(half_count):
        ring_forward(1, step)
    for copy in vscatter + vgather + square_copies(0) + square_copies(1):
        copy.wait_send()
    for at in range(pairs):
        for copy in oscatter[at] + ogather[at]:
            copy.wait_send()
    for mat in range(2):
        for step in range(half_count):
            for way in range(2):
                ring_copy(mat, step, way, False).wait_send()


def body(
    query_rows, key_rows, value_rows, mix_lambda, head_gain, out_cotangent, layer_input,
    value_cotangent, out_weight, value_weight, out_basis, value_basis, out_first, out_second,
    value_first, value_second,
):
    fs_count = lax.axis_size("fs")
    tp_count = lax.axis_size("tp")
    seq_len, cols = query_rows.shape
    width, rank = out_basis.shape
    row_share = value_weight.shape[0]
    rank_share = rank // fs_count
    heads = mix_lambda.shape[0]
    pairs = heads // PAIR
    blocks = seq_len // TILE
    half_count = fs_count // 2
    dma = pltpu.SemaphoreType.DMA
    like = lambda a: jax.ShapeDtypeStruct(a.shape, a.dtype)
    vmem = lambda a: pltpu.VMEM(a.shape, a.dtype)
    anywhere = pl.BlockSpec(memory_space=pl.ANY)
    return pl.pallas_call(
        functools.partial(step_kernel, fs_count, tp_count),
        out_shape=(
            like(out_weight), like(value_weight), like(out_weight), like(value_weight),
            jax.ShapeDtypeStruct((cols, width), BF16),
            jax.ShapeDtypeStruct((width, cols), BF16),
            like(out_first), like(out_second), like(value_first), like(value_second),
        ),
        in_specs=[
            pl.BlockSpec(memory_space=pltpu.SMEM), pl.BlockSpec(memory_space=pltpu.VMEM),
        ] + [anywhere] * 14,
        out_specs=tuple([pl.BlockSpec(memory_space=pltpu.VMEM)] * 10),
        scratch_shapes=[
            vmem(query_rows), vmem(key_rows), vmem(value_rows), vmem(value_cotangent),
            vmem(out_basis), vmem(value_basis), vmem(out_weight), vmem(value_weight),
            vmem(out_first), vmem(out_second), vmem(value_first), vmem(value_second),
            pltpu.VMEM((SLOTS, TILE, width), BF16),
            pltpu.VMEM((seq_len, TILE), F32),
            pltpu.VMEM((seq_len, TILE), F32),
            pltpu.VMEM((seq_len, TILE), BF16),
            pltpu.VMEM((heads, DV, seq_len), BF16),
            pltpu.VMEM((rank, width), BF16),
            pltpu.VMEM((rank, width), BF16),
            pltpu.VMEM((blocks, rank, TILE), BF16),
            pltpu.VMEM((blocks, rank, TILE), BF16),
            pltpu.VMEM((DV, DV), F32),
            pltpu.VMEM((TILE, TILE), F32),
            pltpu.VMEM((rank, cols), F32),
            pltpu.VMEM((pairs, rank, PAIR * DV), F32),
            pltpu.VMEM((fs_count - 1, rank_share, cols), F32),
            pltpu.VMEM((pairs, fs_count - 1, rank_share, PAIR * DV), F32),
            pltpu.VMEM((rank, cols), F32),
            pltpu.VMEM((pairs, rank, PAIR * DV), F32),
            pltpu.VMEM((2, 8, 128), F32),
            pltpu.VMEM((2, tp_count - 1, 8, 128), F32),
            dma((12,)), dma((SLOTS,)),
            dma((fs_count - 1,)), dma((fs_count - 1,)),
            dma((pairs, fs_count - 1)), dma((pairs, fs_count - 1)),
            dma((fs_count - 1,)), dma((fs_count - 1,)),
            dma((pairs, fs_count - 1)), dma((pairs, fs_count - 1)),
            dma((2, tp_count - 1)), dma((2, tp_count - 1)),
            dma((2, 2, half_count)), dma((2, 2, half_count)),
        ],
        compiler_params=pltpu.CompilerParams(
            collective_id=0, has_side_effects=True, vmem_limit_bytes=62 * 1024 * 1024
        ),
        name="step",
    )(
        mix_lambda, head_gain.reshape(1, DV), query_rows, key_rows, value_rows, out_cotangent,
        layer_input, value_cotangent, out_basis, value_basis, out_weight, value_weight,
        out_first, out_second, value_first, value_second,
    )


def solution(mesh):
    placed = (
        P("fs", "tp"),
        P("fs", "tp"),
        P("fs", "tp"),
        P("tp"),
        P(),
        P("fs", None),
        P("fs", None),
        P("fs", "tp"),
        P("tp", "fs"),
        P("fs", "tp"),
        P(),
        P(),
        P("fs", "tp"),
        P("fs", "tp"),
        P("fs", "tp"),
        P("fs", "tp"),
    )
    return jax.shard_map(
        body,
        mesh=mesh,
        in_specs=placed,
        out_specs=(
            P("tp", "fs"),
            P("fs", "tp"),
            P("tp", "fs"),
            P("fs", "tp"),
            P("tp", None),
            P(None, "tp"),
            P("fs", "tp"),
            P("fs", "tp"),
            P("fs", "tp"),
            P("fs", "tp"),
        ),
        check_vma=False,
    )
```

time: 182 us -> 145 us (0.80)
  Pallas kernels: 167 us -> 133 us
  local copies, waits for them, and re-layouts: 13.9 us -> 11.7 us
    pallas_call x2 -> x1, Pallas kernels: 167 us -> 133 us  [body(): pl.pallas_call(functools.partial(step_kernel, fs_count, tp_count), out_sh...]
    unnamed x30 -> x26, local copies, waits for them, and re-layouts: 11.5 us -> 11.7 us
where the time goes in v1:
time: 145 us
  Pallas kernels  133 us (92%)
  local copies, waits for them, and re-layouts  11.7 us (8%)
    pallas_call x1, Pallas kernels, body(): pl.pallas_call(functools.partial(step_kernel, fs_count, tp_count), out_sh...  133 us
    unnamed x26, local copies, waits for them, and re-layouts  11.7 us

profile of v1, /device:TPU:0, one launch (start us, length us, event | category | flops | bytes accessed | tf_op | source)
XLA Modules:
  0.0 145.3 jit_solution(5620664765212967333)
XLA Ops:
  0.6 132.9 %step.1 = (f32[512,256]{1,0:T(8,128)}, f32[256,512]{1,0:T(8,128)}, f32[512,256]{1,0:T(8,128)}, f32[256,512]{1,0:T(8,128)}, bf16[512,2048]{1,0:T(8,128)(2,1)}, /*...) custom-call(f32[4]{0:T(128)} %lam_ref.1, ...), custom_call_target="tpu_custom_call" | custom-call | tf_op jit(solution)/shard_map/step/pallas_call | solution.py:470
  133.6 0.0 copy-start.3
  133.6 0.0 copy-start.2
  133.6 0.0 copy-start.1
  133.6 2.0 %copy.36 = f32[512,256]{1,0:T(8,128)} copy(f32[512,256]{1,0:T(8,128)} %get-tuple-element.20) | data formatting | bytes 1048576
  135.6 1.9 %copy.37 = f32[256,512]{1,0:T(8,128)} copy(f32[256,512]{1,0:T(8,128)} %get-tuple-element.21) | data formatting | bytes 1048576
  137.5 0.0 copy-done.3
  137.5 0.8 copy.38
  138.3 0.0 copy-done.2
  138.3 0.8 copy.39
  139.1 0.0 copy-done.1
  139.1 0.0 copy-start
  139.1 1.3 copy.40
  140.4 1.0 copy-done
  141.4 0.0 copy-start.7
  141.4 0.0 copy-start.6
  141.4 0.0 copy-start.5
  141.4 0.0 copy-start.4
  141.4 1.3 copy.41
  142.7 0.0 copy-done.7
  142.7 0.6 copy.42
  143.4 0.0 copy-done.6
  143.4 0.6 copy.43
  144.0 0.0 copy-done.5
  144.0 0.6 copy.44
  144.6 0.0 copy-done.4
  144.6 0.6 copy.45
Async XLA Ops:
  133.6 3.9 %copy-start.3 = (f32[512,256]{1,0:T(8,128)S(1)}, f32[512,256]{1,0:T(8,128)}, u32[]{:S(2)}) copy-start(f32[512,256]{1,0:T(8,128)} %get-tuple-element.22) | copy-start | bytes 1572868
  133.6 4.7 %copy-start.2 = (f32[256,512]{1,0:T(8,128)S(1)}, f32[256,512]{1,0:T(8,128)}, u32[]{:S(2)}) copy-start(f32[256,512]{1,0:T(8,128)} %get-tuple-element.23) | copy-start | bytes 1572868
  133.6 5.5 %copy-start.1 = (bf16[512,2048]{1,0:T(8,128)(2,1)S(1)}, bf16[512,2048]{1,0:T(8,128)(2,1)}, u32[]{:S(2)}) copy-start(bf16[512,2048]{1,0:T(8,128)(2,1)} %get-tuple-element.24) | copy-start | bytes 6291460
  139.1 2.3 %copy-start = (bf16[2048,512]{1,0:T(8,128)(2,1)S(1)}, bf16[2048,512]{1,0:T(8,128)(2,1)}, u32[]{:S(2)}) copy-start(bf16[2048,512]{1,0:T(8,128)(2,1)} %get-tuple-element.25) | copy-start | bytes 6291460
  141.4 1.3 copy-start.7
  141.4 2.0 %copy-start.6 = (f32[32,512]{1,0:T(8,128)S(1)}, f32[32,512]{1,0:T(8,128)}, u32[]{:S(2)}) copy-start(f32[32,512]{1,0:T(8,128)} %get-tuple-element.27) | copy-start | bytes 196612
  141.4 2.6 %copy-start.5 = (f32[32,512]{1,0:T(8,128)S(1)}, f32[32,512]{1,0:T(8,128)}, u32[]{:S(2)}) copy-start(f32[32,512]{1,0:T(8,128)} %get-tuple-element.28) | copy-start | bytes 196612
  141.4 3.2 %copy-start.4 = (f32[32,512]{1,0:T(8,128)S(1)}, f32[32,512]{1,0:T(8,128)}, u32[]{:S(2)}) copy-start(f32[32,512]{1,0:T(8,128)} %get-tuple-element.29) | copy-start | bytes 196612

commit v2 on v1

--- a/solution.py
+++ b/solution.py
@@ -20,6 +20,7 @@
 LEARN_RATE = 0.01
 TILE = 256
 SLOTS = 4
+EARLY = 4
 PAIR = 2
 LOG2E = 1.4426950408889634
 F32 = jnp.float32
@@ -51,13 +52,13 @@
     fs_count, tp_count,
     lam_ref, gain_ref, query_h, key_h, value_h, cot_h, input_h, vcot_h, obasis_h, vbasis_h,
     oweight_h, vweight_h, ofirst_h, osecond_h, vfirst_h, vsecond_h,
-    ostep, vstep, onew, vnew, ocopy, vcopy, ofirst_new, osecond_new, vfirst_new, vsecond_new,
+    vproj_o, oproj_o, vdirs_o, odirs_o, clips_o, vcopy_o, ocopy_o, early_o,
     query_v, key_v, value_v, vcot_v, obasis_v, vbasis_v, oweight, vweight,
-    ofirst, osecond, vfirst, vsecond, chunks,
+    ofirst, osecond, vfirst, vsecond, chunks, vstep, ostep, vcopy, ocopy, early_w, clips,
     score_one, score_two, mix_ref, value_t, obasis_t, vbasis_t, cb_high, cb_low, gain_t, tri,
     vproj, oproj, vgot, ogot, vdirs, odirs, squares, squares_got,
     load_sem, chunk_sem, vs_send, vs_recv, os_send, os_recv, vg_send, vg_recv, og_send, og_recv,
-    sq_send, sq_recv, ring_send, ring_recv,
+    sq_send, sq_recv, ring_send, ring_recv, out_sem, block_sem,
 ):
     me = lax.axis_index("fs")
     my_tp = lax.axis_index("tp")
@@ -68,6 +69,7 @@
     blocks = seq_len // TILE
     pairs = oproj.shape[0]
     wide = PAIR * DV
+    early_rows = early_w.shape[0]
     mesh_ids = pl.DeviceIdType.MESH
 
     def fs_peer(gap):
@@ -105,13 +107,19 @@
     early.append(load(1, vcot_h, vcot_v))
     chunk_copy(input_h, SLOTS - 1, SLOTS - 1).start()
     early.append(load(2, obasis_h, obasis_v))
-    attention = [
-        load(3, query_h, query_v), load(4, key_h, key_v), load(5, value_h, value_v),
+    early_own = load(
+        12, oweight_h.at[pl.ds(0, early_rows)], early_w.at[:, share(me, row_share)]
+    )
+    later = [
+        (3, query_h, query_v), (4, key_h, key_v), (5, value_h, value_v),
+        (6, vfirst_h, vfirst), (7, vsecond_h, vsecond), (8, ofirst_h, ofirst),
+        (9, osecond_h, osecond), (10, vweight_h, vweight), (11, oweight_h, oweight),
     ]
-    late = [
-        load(6, vfirst_h, vfirst), load(7, vsecond_h, vsecond), load(8, ofirst_h, ofirst),
-        load(9, osecond_h, osecond), load(10, vweight_h, vweight), load(11, oweight_h, oweight),
+    later = [
+        pltpu.make_async_copy(source, target, load_sem.at[index])
+        for index, source, target in later
     ]
+    attention, late = later[:3], later[3:]
 
     key_pos = lax.broadcasted_iota(jnp.int32, (TILE, TILE), 0)
     query_pos = lax.broadcasted_iota(jnp.int32, (TILE, TILE), 1)
@@ -119,30 +127,6 @@
     gain_t[...] = jnp.broadcast_to(gain_ref[...], (DV, DV)).T
     vproj[...] = jnp.zeros_like(vproj)
     oproj[...] = jnp.zeros_like(oproj)
-
-    early[0].wait()
-    vbasis_t[...] = vbasis_v[...].T
-    early[1].wait()
-
-    def value_block(at, carry):
-        slot = lax.rem(at, SLOTS)
-        chunk_copy(input_h, at, slot).wait()
-        high, low = split_two(dot_f32(vbasis_t[...], chunks[slot], ((1,), (1,))))
-        vcot = vcot_v[share(at, TILE), :]
-        vproj[...] += dot_f32(high, vcot) + dot_f32(low, vcot)
-
-        @pl.when(at < blocks - SLOTS)
-        def _():
-            chunk_copy(input_h, at + SLOTS, slot).start()
-
-        @pl.when(at >= blocks - SLOTS)
-        def _():
-            chunk_copy(cot_h, at - (blocks - SLOTS), slot).start()
-
-        return carry
-
-    lax.fori_loop(0, blocks, value_block, 0)
-    pl.semaphore_wait(barrier, fs_count + tp_count - 2)
 
     def exchange(source, target, send, recv):
         copies = []
@@ -235,8 +219,10 @@
     def ring_block(mat, at, split):
         if mat == 0:
             return vcopy.at[halved(at * row_share, row_share, split)]
-        rows = slice(None) if split is None else pl.ds(split * (cols // 2), cols // 2)
-        return ocopy.at[rows, share(at, row_share)]
+        held = ocopy if mat == 1 else early_w
+        count = held.shape[0]
+        rows = slice(None) if split is None else pl.ds(split * (count // 2), count // 2)
+        return held.at[rows, share(at, row_share)]
 
     def ring_copy(mat, step, way, arriving):
         back = step + 1 if arriving else step
@@ -261,6 +247,25 @@
             if step + 1 < half_count:
                 ring_copy(mat, step + 1, way, False).start()
 
+    sends = [
+        (vproj.at[share(me, rank_share)], vproj_o), (vdirs, vdirs_o),
+    ]
+    for at in range(pairs):
+        sends += [
+            (oproj.at[at, share(me, rank_share)], oproj_o.at[at]), (odirs.at[at], odirs_o.at[at]),
+        ]
+    sends += [(clips, clips_o), (vcopy, vcopy_o), (early_w, early_o)]
+
+    def out_copy(index):
+        source, target = sends[index]
+        return pltpu.make_async_copy(source, target, out_sem.at[index])
+
+    def block_copy(at):
+        columns = share(at, row_share)
+        return pltpu.make_async_copy(
+            ocopy.at[:, columns], ocopy_o.at[:, columns], block_sem.at[at]
+        )
+
     def value_moments():
         for copy in late:
             copy.wait()
@@ -268,25 +273,25 @@
         for gap in range(1, fs_count):
             vscatter[gap - 1].wait_recv()
             proj += vgot[gap - 1]
-        new_first, new_second, direction = moment_step(proj, vfirst[...], vsecond[...])
+        direction = moment_step(proj, vfirst[...], vsecond[...])[2]
         vdirs[share(me, rank_share), :] = direction
         start_all(vgather)
-        vfirst_new[...] = new_first
-        vsecond_new[...] = new_second
+        vproj[share(me, rank_share), :] = proj
+        out_copy(0).start()
 
     def value_squares():
         for copy in vgather:
             copy.wait_recv()
         put_squares(0, [vdirs[...]])
+        out_copy(1).start()
         high, low = split_two(vdirs[...])
         rows = vbasis_v[share(me, row_share), :]
         vstep[...] = dot_f32(rows, high) + dot_f32(rows, low)
 
     def value_update():
-        step = clip_of(0) * vstep[...]
-        vstep[...] = step
-        weight = vweight[...] - LEARN_RATE * step
-        vnew[...] = weight
+        clip = clip_of(0)
+        clips[0] = jnp.broadcast_to(clip, (8, 128))
+        weight = vweight[...] - LEARN_RATE * (clip * vstep[...])
         vcopy[share(me, row_share), :] = weight.astype(BF16)
         ring_begin(0)
 
@@ -296,15 +301,16 @@
         for gap in range(1, fs_count):
             oscatter[at][gap - 1].wait_recv()
             proj += ogot[at, gap - 1]
-        new_first, new_second, direction = moment_step(proj, ofirst[:, span], osecond[:, span])
+        direction = moment_step(proj, ofirst[:, span], osecond[:, span])[2]
         odirs[at, share(me, rank_share), :] = direction
         start_all(ogather[at])
-        ofirst_new[:, span] = new_first
-        osecond_new[:, span] = new_second
+        oproj[at, share(me, rank_share), :] = proj
+        out_copy(2 + 2 * at).start()
 
     def out_arrived(at):
         for copy in ogather[at]:
             copy.wait_recv()
+        out_copy(3 + 2 * at).start()
 
     def out_step(at):
         rows = obasis_v[share(me, row_share), :]
@@ -316,13 +322,47 @@
     def out_update():
         put_squares(1, [odirs[at] for at in range(pairs)])
         out_step(pairs - 1)
-        step = clip_of(1) * ostep[...]
-        ostep[...] = step
-        weight = oweight[...] - LEARN_RATE * step
-        onew[...] = weight
+        clip = clip_of(1)
+        clips[1] = jnp.broadcast_to(clip, (8, 128))
+        rows = pl.ds(early_rows, cols - early_rows)
+        weight = oweight[rows, :] - LEARN_RATE * (clip * ostep[rows, :])
         ocopy[:, share(me, row_share)] = weight.astype(BF16)
         ring_begin(1)
-
+        out_copy(2 + 2 * pairs).start()
+        block_copy(me).start()
+
+    def enter():
+        pl.semaphore_wait(barrier, fs_count + tp_count - 2)
+        early_own.wait()
+        ring_begin(2)
+
+    early[0].wait()
+    vbasis_t[...] = vbasis_v[...].T
+    early[1].wait()
+
+    def value_block(at, carry):
+        slot = lax.rem(at, SLOTS)
+        chunk_copy(input_h, at, slot).wait()
+        high, low = split_two(dot_f32(vbasis_t[...], chunks[slot], ((1,), (1,))))
+        vcot = vcot_v[share(at, TILE), :]
+        vproj[...] += dot_f32(high, vcot) + dot_f32(low, vcot)
+
+        @pl.when(at < blocks - SLOTS)
+        def _():
+            chunk_copy(input_h, at + SLOTS, slot).start()
+
+        @pl.when(at >= blocks - SLOTS)
+        def _():
+            chunk_copy(cot_h, at - (blocks - SLOTS), slot).start()
+
+        @pl.when(at == SLOTS)
+        def _():
+            start_all(later)
+
+        pl.when(at == 2)(enter)
+        return carry
+
+    lax.fori_loop(0, blocks, value_block, 0)
     start_all(vscatter)
 
     early[2].wait()
@@ -342,6 +382,7 @@
         return carry
 
     lax.fori_loop(0, blocks, cot_block, 0)
+    ring_forward(2, 0)
     for copy in attention:
         copy.wait()
     for head in range(pairs * PAIR):
@@ -406,17 +447,26 @@
         events.setdefault((pair, item), []).append(action)
 
     last = 2 * blocks
-    at = (8, 13, 14, 17, 21, 24, 27)
+    at = (11, 17, 19, 26, 30)
     actions = [value_moments, value_squares, value_update] + [
-        functools.partial(ring_forward, 0, step) for step in range(half_count)
+        functools.partial(ring_forward, 0, step) for step in range(2)
     ]
+
+    def early_done():
+        for step in range(3, half_count):
+            ring_forward(2, step)
+        out_copy(4 + 2 * pairs).start()
+
+    plan(0, 8, functools.partial(ring_forward, 2, 1))
+    plan(0, 12, functools.partial(ring_forward, 2, 2))
+    plan(0, 15, early_done)
     for tick, action in zip(at, actions):
         plan(tick // last, tick % last, action)
     for pair in range(pairs - 1):
-        plan(pair + 1, 2, functools.partial(start_all, oscatter[pair]))
-        plan(pair + 1, 10, functools.partial(out_moments, pair))
-        plan(pair + 1, 14, functools.partial(out_arrived, pair))
-        plan(pair + 1, 14, functools.partial(out_step, pair))
+        plan(pair + 1, 0, functools.partial(start_all, oscatter[pair]))
+        plan(pair + 1, 8, functools.partial(out_moments, pair))
+        plan(pair + 1, 15, functools.partial(out_arrived, pair))
+        plan(pair + 1, 15, functools.partial(out_step, pair))
 
     def pair_items(pair, carry):
         for item in range(last):
@@ -432,20 +482,111 @@
         if pair >= pairs:
             for action in events[(pair, item)]:
                 action()
+    for step in range(2, half_count - 1):
+        ring_forward(0, step)
     out_moments(pairs - 1)
+    ring_forward(0, half_count - 1)
+    out_copy(3 + 2 * pairs).start()
     out_arrived(pairs - 1)
     out_update()
     for step in range(half_count):
         ring_forward(1, step)
+        back = step + 1
+        if step < half_count - 1:
+            block_copy(owner(place - back)).start()
+        block_copy(owner(place + back)).start()
     for copy in vscatter + vgather + square_copies(0) + square_copies(1):
         copy.wait_send()
     for at in range(pairs):
         for copy in oscatter[at] + ogather[at]:
             copy.wait_send()
-    for mat in range(2):
+    for mat in range(3):
         for step in range(half_count):
             for way in range(2):
                 ring_copy(mat, step, way, False).wait_send()
+    for index in range(len(sends)):
+        out_copy(index).wait()
+    for at in range(fs_count):
+        block_copy(at).wait()
+
+
+def finish_kernel(*refs):
+    inputs, outputs, scratch = refs[:16], refs[16:26], refs[26:]
+    in_sem, out_sem = scratch[-2:]
+    held, results, early_copy = scratch[:16], scratch[16:24], scratch[24]
+    (
+        clips, vproj, oproj, ofirst, osecond, vfirst, vsecond, vdirs, odirs, obasis, vbasis,
+        oweight, vweight, early_w, vcopy, ocopy,
+    ) = held
+    (
+        ostep_o, vstep_o, onew_o, vnew_o, ocopy_o, vcopy_o, ofirst_o, osecond_o, vfirst_o,
+        vsecond_o,
+    ) = outputs
+    ostep, vstep, onew, vnew, ofirst_new, osecond_new, vfirst_new, vsecond_new = results
+    me = lax.axis_index("fs")
+    row_share = vweight.shape[0]
+    rows = pl.ds(pl.multiple_of(me * row_share, row_share), row_share)
+    early_rows = early_w.shape[0]
+    arrivals = [
+        pltpu.make_async_copy(source, target, in_sem.at[index])
+        for index, (source, target) in enumerate(zip(inputs, held))
+    ]
+    for copy in arrivals:
+        copy.start()
+    leaving = []
+
+    def leave(source, target):
+        copy = pltpu.make_async_copy(source, target, out_sem.at[len(leaving)])
+        copy.start()
+        leaving.append(copy)
+
+    for index in range(14):
+        arrivals[index].wait()
+    clip_value = clips[0, :1, :1]
+    clip_out = clips[1, :1, :1]
+    pairs, rank, wide = odirs.shape
+    out_parts = [split_two(odirs[at]) for at in range(pairs)]
+    for start in range(0, early_rows, wide):
+        count = min(wide, early_rows - start)
+        high, low = out_parts[start // wide]
+        high, low = high[:, :count], low[:, :count]
+        step = dot_f32(high, obasis[...], ((0,), (1,))) + dot_f32(low, obasis[...], ((0,), (1,)))
+        span = slice(start, start + count)
+        early_copy[span, :] = (early_w[span, :] - LEARN_RATE * (clip_out * step)).astype(BF16)
+    leave(early_copy, ocopy_o.at[pl.ds(0, early_rows)])
+    arrivals[14].wait()
+    leave(vcopy, vcopy_o)
+    arrivals[15].wait()
+    leave(ocopy, ocopy_o.at[pl.ds(early_rows, ocopy.shape[0])])
+    high, low = split_two(vdirs[...])
+    step = clip_value * (dot_f32(vbasis[rows, :], high) + dot_f32(vbasis[rows, :], low))
+    vstep[...] = step
+    leave(vstep, vstep_o)
+    vnew[...] = vweight[...] - LEARN_RATE * step
+    leave(vnew, vnew_o)
+    for at in range(pairs):
+        high, low = out_parts[at]
+        step = clip_out * (
+            dot_f32(high, obasis[rows, :], ((0,), (1,)))
+            + dot_f32(low, obasis[rows, :], ((0,), (1,)))
+        )
+        span = slice(at * wide, (at + 1) * wide)
+        ostep[span, :] = step
+        onew[span, :] = oweight[span, :] - LEARN_RATE * step
+        moments = moment_step(oproj[at], ofirst[:, span], osecond[:, span])
+        ofirst_new[:, span] = moments[0]
+        osecond_new[:, span] = moments[1]
+    moments = moment_step(vproj[...], vfirst[...], vsecond[...])
+    vfirst_new[...] = moments[0]
+    vsecond_new[...] = moments[1]
+    leave(ostep, ostep_o)
+    leave(onew, onew_o)
+    leave(ofirst_new, ofirst_o)
+    leave(osecond_new, osecond_o)
+    leave(vfirst_new, vfirst_o)
+    leave(vsecond_new, vsecond_o)
+    for copy in leaving:
+        copy.wait()
 
 
 def body(
@@ -467,23 +608,33 @@
     like = lambda a: jax.ShapeDtypeStruct(a.shape, a.dtype)
     vmem = lambda a: pltpu.VMEM(a.shape, a.dtype)
     anywhere = pl.BlockSpec(memory_space=pl.ANY)
-    return pl.pallas_call(
+    early_rows = cols // EARLY
+    early_shape = (early_rows, width)
+    rest_shape = (cols - early_rows, width)
+    vproj, oproj, vdirs, odirs, clips, vcopy, ocopy, early_w = pl.pallas_call(
         functools.partial(step_kernel, fs_count, tp_count),
         out_shape=(
-            like(out_weight), like(value_weight), like(out_weight), like(value_weight),
-            jax.ShapeDtypeStruct((cols, width), BF16),
+            like(value_first),
+            jax.ShapeDtypeStruct((pairs, rank_share, PAIR * DV), F32),
+            jax.ShapeDtypeStruct((rank, cols), F32),
+            jax.ShapeDtypeStruct((pairs, rank, PAIR * DV), F32),
+            jax.ShapeDtypeStruct((2, 8, 128), F32),
             jax.ShapeDtypeStruct((width, cols), BF16),
-            like(out_first), like(out_second), like(value_first), like(value_second),
+            jax.ShapeDtypeStruct(rest_shape, BF16),
+            jax.ShapeDtypeStruct(early_shape, F32),
         ),
         in_specs=[
             pl.BlockSpec(memory_space=pltpu.SMEM), pl.BlockSpec(memory_space=pltpu.VMEM),
         ] + [anywhere] * 14,
-        out_specs=tuple([pl.BlockSpec(memory_space=pltpu.VMEM)] * 10),
+        out_specs=tuple([anywhere] * 8),
         scratch_shapes=[
             vmem(query_rows), vmem(key_rows), vmem(value_rows), vmem(value_cotangent),
             vmem(out_basis), vmem(value_basis), vmem(out_weight), vmem(value_weight),
             vmem(out_first), vmem(out_second), vmem(value_first), vmem(value_second),
             pltpu.VMEM((SLOTS, TILE, width), BF16),
+            vmem(value_weight), vmem(out_weight), pltpu.VMEM((width, cols), BF16),
+            pltpu.VMEM(rest_shape, BF16), pltpu.VMEM(early_shape, F32),
+            pltpu.VMEM((2, 8, 128), F32),
             pltpu.VMEM((seq_len, TILE), F32),
             pltpu.VMEM((seq_len, TILE), F32),
             pltpu.VMEM((seq_len, TILE), BF16),
@@ -502,13 +653,14 @@
             pltpu.VMEM((pairs, rank, PAIR * DV), F32),
             pltpu.VMEM((2, 8, 128), F32),
             pltpu.VMEM((2, tp_count - 1, 8, 128), F32),
-            dma((12,)), dma((SLOTS,)),
+            dma((13,)), dma((SLOTS,)),
             dma((fs_count - 1,)), dma((fs_count - 1,)),
             dma((pairs, fs_count - 1)), dma((pairs, fs_count - 1)),
             dma((fs_count - 1,)), dma((fs_count - 1,)),
             dma((pairs, fs_count - 1)), dma((pairs, fs_count - 1)),
             dma((2, tp_count - 1)), dma((2, tp_count - 1)),
-            dma((2, 2, half_count)), dma((2, 2, half_count)),
+            dma((3, 2, half_count)), dma((3, 2, half_count)),
+            dma((5 + 2 * pairs,)), dma((fs_count,)),
         ],
         compiler_params=pltpu.CompilerParams(
             collective_id=0, has_side_effects=True, vmem_limit_bytes=62 * 1024 * 1024
@@ -519,6 +671,27 @@
         layer_input, value_cotangent, out_basis, value_basis, out_weight, value_weight,
         out_first, out_second, value_first, value_second,
     )
+    results = (
+        like(out_weight), like(value_weight), like(out_weight), like(value_weight),
+        jax.ShapeDtypeStruct((cols, width), BF16),
+        jax.ShapeDtypeStruct((width, cols), BF16),
+        like(out_first), like(out_second), like(value_first), like(value_second),
+    )
+    operands = (
+        clips, vproj, oproj, out_first, out_second, value_first, value_second, vdirs, odirs,
+        out_basis, value_basis, out_weight, value_weight, early_w, vcopy, ocopy,
+    )
+    return pl.pallas_call(
+        finish_kernel,
+        out_shape=results,
+        in_specs=[anywhere] * len(operands),
+        out_specs=tuple([anywhere] * len(results)),
+        scratch_shapes=[vmem(a) for a in operands + results[:4] + results[6:]] + [
+            pltpu.VMEM(early_shape, BF16), dma((len(operands),)), dma((11,)),
+        ],
+        compiler_params=pltpu.CompilerParams(vmem_limit_bytes=62 * 1024 * 1024),
+        name="finish",
+    )(*operands)
 
 
 def solution(mesh):

time: 145 us -> 129 us (0.89)
  local copies, waits for them, and re-layouts: 11.7 us -> 0 us
  Pallas kernels: 133 us -> 128 us
    unnamed x26 -> x0, local copies, waits for them, and re-layouts: 11.7 us -> none
    pallas_call x1, Pallas kernels: 133 us -> 122 us  [body(): pl.pallas_call(functools.partial(step_kernel, fs_count, tp_count), out_sh...]
    pallas_call x0 -> x1, Pallas kernels: none -> 6.53 us  [body(): pl.pallas_call(finish_kernel, out_shape=results, in_specs=[anywhere] * le...]
where the time goes in v2:
time: 129 us
  Pallas kernels  128 us (99%)
    pallas_call x1, Pallas kernels, body(): pl.pallas_call(functools.partial(step_kernel, fs_count, tp_count), out_sh...  122 us
    pallas_call x1, Pallas kernels, body(): pl.pallas_call(finish_kernel, out_shape=results, in_specs=[anywhere] * le...  6.53 us

profile of v2, /device:TPU:0, one launch (start us, length us, event | category | flops | bytes accessed | tf_op | source)
XLA Modules:
  0.0 129.1 jit_solution(13678858721669912262)
XLA Ops:
  0.6 121.7 %step.1 = (f32[32,512]{1,0:T(8,128)}, f32[2,32,256]{2,1,0:T(8,128)}, f32[256,512]{1,0:T(8,128)}, f32[2,256,256]{2,1,0:T(8,128)}, f32[2,8,128]{2,1,0:T(8,128)}, /...) custom-call(f32[4]{0:T(128)} %lam_ref.1, f32[1,128]{1,0:T(1,128)} %bitcast.1, ...), custom_call_target="tpu_custom_call" | custom-call | tf_op jit(solution)/shard_map/step/pallas_call | solution.py:614
  122.4 6.5 %finish.1 = (f32[512,256]{1,0:T(8,128)}, f32[256,512]{1,0:T(8,128)}, f32[512,256]{1,0:T(8,128)}, f32[256,512]{1,0:T(8,128)}, bf16[512,2048]{1,0:T(8,128)(2,1)}, ...) custom-call(f32[2,8,128]{2,1,0:T(8,128)} %get-tuple-element.18.refs_, ...), custom_call_target="tpu_custom_call" | custom-call | tf_op jit(solution)/shard_map/finish/pallas_call | solution.py:684

commit v3 on v2

--- a/solution.py
+++ b/solution.py
@@ -20,7 +20,8 @@
 LEARN_RATE = 0.01
 TILE = 256
 SLOTS = 4
-EARLY = 4
+EARLY = 8
+HELD = 4
 PAIR = 2
 LOG2E = 1.4426950408889634
 F32 = jnp.float32
@@ -55,9 +56,9 @@
     vproj_o, oproj_o, vdirs_o, odirs_o, clips_o, vcopy_o, ocopy_o, early_o,
     query_v, key_v, value_v, vcot_v, obasis_v, vbasis_v, oweight, vweight,
     ofirst, osecond, vfirst, vsecond, chunks, vstep, ostep, vcopy, ocopy, early_w, clips,
-    score_one, score_two, mix_ref, value_t, obasis_t, vbasis_t, cb_high, cb_low, gain_t, tri,
+    scores, peak_ref, sum_ref, mix_ref, value_t, obasis_t, vbasis_t, cb_high, cb_low, gain_t, tri,
     vproj, oproj, vgot, ogot, vdirs, odirs, squares, squares_got,
-    load_sem, chunk_sem, vs_send, vs_recv, os_send, os_recv, vg_send, vg_recv, og_send, og_recv,
+    load_sem, chunk_sem, vs_send, vs_recv, os_send, os_recv,
     sq_send, sq_recv, ring_send, ring_recv, out_sem, block_sem,
 ):
     me = lax.axis_index("fs")
@@ -148,10 +149,6 @@
         lambda peer: vproj.at[share(peer, rank_share)], lambda gap: vgot.at[gap - 1],
         vs_send, vs_recv,
     )
-    vgather = exchange(
-        lambda peer: vdirs.at[share(me, rank_share)],
-        lambda gap: vdirs.at[share(me, rank_share)], vg_send, vg_recv,
-    )
     oscatter = [
         exchange(
             lambda peer, at=at: oproj.at[at, share(peer, rank_share)],
@@ -159,15 +156,6 @@
         )
         for at in range(pairs)
     ]
-    ogather = [
-        exchange(
-            lambda peer, at=at: odirs.at[at, share(me, rank_share)],
-            lambda gap, at=at: odirs.at[at, share(me, rank_share)],
-            og_send.at[at], og_recv.at[at],
-        )
-        for at in range(pairs)
-    ]
-
     def start_all(copies):
         for copy in copies:
             copy.start()
@@ -219,6 +207,10 @@
     def ring_block(mat, at, split):
         if mat == 0:
             return vcopy.at[halved(at * row_share, row_share, split)]
+        if mat == 3:
+            return vdirs.at[halved(at * rank_share, rank_share, split)]
+        if mat > 3:
+            return odirs.at[mat - 4, halved(at * rank_share, rank_share, split)]
         held = ocopy if mat == 1 else early_w
         count = held.shape[0]
         rows = slice(None) if split is None else pl.ds(split * (count // 2), count // 2)
@@ -275,13 +267,13 @@
             proj += vgot[gap - 1]
         direction = moment_step(proj, vfirst[...], vsecond[...])[2]
         vdirs[share(me, rank_share), :] = direction
-        start_all(vgather)
+        ring_begin(3)
         vproj[share(me, rank_share), :] = proj
         out_copy(0).start()
 
     def value_squares():
-        for copy in vgather:
-            copy.wait_recv()
+        for step in range(3, half_count):
+            ring_forward(3, step)
         put_squares(0, [vdirs[...]])
         out_copy(1).start()
         high, low = split_two(vdirs[...])
@@ -303,13 +295,11 @@
             proj += ogot[at, gap - 1]
         direction = moment_step(proj, ofirst[:, span], osecond[:, span])[2]
         odirs[at, share(me, rank_share), :] = direction
-        start_all(ogather[at])
+        ring_begin(4 + at)
         oproj[at, share(me, rank_share), :] = proj
         out_copy(2 + 2 * at).start()
 
     def out_arrived(at):
-        for copy in ogather[at]:
-            copy.wait_recv()
         out_copy(3 + 2 * at).start()
 
     def out_step(at):
@@ -388,50 +378,70 @@
     for head in range(pairs * PAIR):
         value_t[head] = value_v[:, head * DV : (head + 1) * DV].T
 
+    last = PAIR * blocks
     lane = lax.broadcasted_iota(jnp.int32, (TILE, DV), 1)
 
-    def attend(block, pair, which):
-        head = pair * PAIR + which
-        columns = pl.ds(pl.multiple_of(head * DV, DV), DV)
-        lam = lam_ref[head]
-        width = (block + 1) * TILE
+    def head_columns(pair, which):
+        return pl.ds(pl.multiple_of((pair * PAIR + which) * DV, DV), DV)
+
+    def score_steps(item, pair):
+        block, which = divmod(item, PAIR)
+        slot = item % HELD
+        columns = head_columns(pair, which)
         query = query_v[block * TILE : (block + 1) * TILE, columns].astype(F32)
         query = query * (DH ** (-0.5) * LOG2E)
-        parts_one = split_two(jnp.where(lane < DH, query, 0.0))
-        parts_two = split_two(jnp.where(lane < DH, 0.0, query))
-        query_one = jnp.concatenate(parts_one, axis=1)
-        query_two = jnp.concatenate(parts_two, axis=1)
-        peak_one = jnp.full((8, TILE), -jnp.inf, F32)
-        peak_two = peak_one
-        for at in range(0, width, TILE):
-            keys = key_v[at : at + TILE, columns]
+        queries = [
+            jnp.concatenate(split_two(part), axis=1)
+            for part in (jnp.where(lane < DH, query, 0.0), jnp.where(lane < DH, 0.0, query))
+        ]
+        peaks = [jnp.full((8, TILE), -jnp.inf, F32)] * 2
+        for tile in range(block + 1):
+            span = slice(tile * TILE, (tile + 1) * TILE)
+            keys = key_v[span, columns]
             keys = jnp.concatenate([keys, keys], axis=1)
-            one = dot_f32(keys, query_one, ((1,), (1,)))
-            two = dot_f32(keys, query_two, ((1,), (1,)))
-            if at == width - TILE:
-                one = one + tri[...]
-                two = two + tri[...]
-            score_one[at : at + TILE, :] = one
-            score_two[at : at + TILE, :] = two
-            peak_one = jnp.maximum(peak_one, fold_rows(one, jnp.max))
-            peak_two = jnp.maximum(peak_two, fold_rows(two, jnp.max))
-        peak_one = jnp.max(peak_one, axis=0, keepdims=True)
-        peak_two = jnp.max(peak_two, axis=0, keepdims=True)
-        sum_one = jnp.zeros((8, TILE), F32)
-        sum_two = sum_one
-        for at in range(0, width, TILE):
-            one = jnp.exp2(score_one[at : at + TILE, :] - peak_one)
-            two = jnp.exp2(score_two[at : at + TILE, :] - peak_two)
-            score_one[at : at + TILE, :] = one
-            score_two[at : at + TILE, :] = two
-            sum_one += fold_rows(one, jnp.sum)
-            sum_two += fold_rows(two, jnp.sum)
-        rate_one = 1.0 / jnp.sum(sum_one, axis=0, keepdims=True)
-        rate_two = lam / jnp.sum(sum_two, axis=0, keepdims=True)
-        for at in range(0, width, TILE):
-            mix_ref[at : at + TILE, :] = (
-                score_one[at : at + TILE, :] * rate_one - score_two[at : at + TILE, :] * rate_two
+            for which_map in range(2):
+                one = dot_f32(keys, queries[which_map], ((1,), (1,)))
+                if tile == block:
+                    one = one + tri[...]
+                scores[slot, which_map, span, :] = one
+                peaks[which_map] = jnp.maximum(peaks[which_map], fold_rows(one, jnp.max))
+            if tile == block:
+                for which_map in range(2):
+                    peak_ref[slot, which_map] = peaks[which_map]
+            yield
+
+    def exp_steps(item):
+        slot = item % HELD
+        peaks = [
+            jnp.max(peak_ref[slot, which_map], axis=0, keepdims=True) for which_map in range(2)
+        ]
+        sums = [jnp.zeros((8, TILE), F32)] * 2
+        last_tile = item // PAIR
+        for tile in range(last_tile + 1):
+            span = slice(tile * TILE, (tile + 1) * TILE)
+            for which_map in range(2):
+                one = jnp.exp2(scores[slot, which_map, span, :] - peaks[which_map])
+                scores[slot, which_map, span, :] = one
+                sums[which_map] += fold_rows(one, jnp.sum)
+            if tile == last_tile:
+                for which_map in range(2):
+                    sum_ref[slot, which_map] = sums[which_map]
+            yield
+
+    def mix_steps(item, pair):
+        block, which = divmod(item, PAIR)
+        slot = item % HELD
+        head = pair * PAIR + which
+        width = (block + 1) * TILE
+        rate_one = 1.0 / jnp.sum(sum_ref[slot, 0], axis=0, keepdims=True)
+        rate_two = lam_ref[head] / jnp.sum(sum_ref[slot, 1], axis=0, keepdims=True)
+        for tile in range(block + 1):
+            span = slice(tile * TILE, (tile + 1) * TILE)
+            mix_ref[span, :] = (
+                scores[slot, 0, span, :] * rate_one - scores[slot, 1, span, :] * rate_two
             ).astype(BF16)
+            if tile < block:
+                yield
         raw = dot_f32(value_t[head, :, :width], mix_ref[:width, :])
         mean_sq = jnp.mean(raw * raw, axis=0, keepdims=True)
         gain = jnp.concatenate([gain_t[...]] * (TILE // DV), axis=1)
@@ -440,52 +450,86 @@
         oproj[pair, :, span] += dot_f32(cb_high[block], out_t, ((1,), (1,))) + dot_f32(
             cb_low[block], out_t, ((1,), (1,))
         )
+        yield
+
+    def together(*steps):
+        live = list(steps)
+        while live:
+            live = [step for step in live if next(step, "done") != "done"]
+
+    def attend(item, pair):
+        before, ahead = (item - 1) % last, (item - 2) % last
+        if item >= 2:
+            together(
+                mix_steps(ahead, pair), exp_steps(before), score_steps(item, pair)
+            )
+            return
+        if item == 1:
+            pl.when(pair > 0)(lambda: together(mix_steps(ahead, pair - 1)))
+            together(exp_steps(before), score_steps(item, pair))
+            return
+        pl.when(pair > 0)(
+            lambda: together(mix_steps(ahead, pair - 1), exp_steps(before))
+        )
+        together(score_steps(item, pair))
 
     events = {}
 
     def plan(pair, item, action):
         events.setdefault((pair, item), []).append(action)
 
-    last = 2 * blocks
-    at = (11, 17, 19, 26, 30)
-    actions = [value_moments, value_squares, value_update] + [
-        functools.partial(ring_forward, 0, step) for step in range(2)
-    ]
+    at = (13, 16, 18, 22, 25, 27)
+    actions = (
+        [value_moments]
+        + [functools.partial(ring_forward, 3, step) for step in range(3)]
+        + [value_squares, value_update]
+    )
 
     def early_done():
         for step in range(3, half_count):
             ring_forward(2, step)
         out_copy(4 + 2 * pairs).start()
 
-    plan(0, 8, functools.partial(ring_forward, 2, 1))
-    plan(0, 12, functools.partial(ring_forward, 2, 2))
-    plan(0, 15, early_done)
+    plan(0, 12, functools.partial(ring_forward, 2, 1))
+    plan(0, 15, functools.partial(ring_forward, 2, 2))
+    plan(1, 4, early_done)
     for tick, action in zip(at, actions):
         plan(tick // last, tick % last, action)
     for pair in range(pairs - 1):
-        plan(pair + 1, 0, functools.partial(start_all, oscatter[pair]))
-        plan(pair + 1, 8, functools.partial(out_moments, pair))
-        plan(pair + 1, 15, functools.partial(out_arrived, pair))
-        plan(pair + 1, 15, functools.partial(out_step, pair))
+        plan(pair + 1, 10, functools.partial(start_all, oscatter[pair]))
+        plan(pair + 1, 15, functools.partial(out_moments, pair))
 
     def pair_items(pair, carry):
         for item in range(last):
             for when in range(pairs):
                 for action in events.get((when, item), []):
                     pl.when(pair == when)(action)
-            attend(item // PAIR, pair, item % PAIR)
+            attend(item, pair)
         return carry
 
     lax.fori_loop(0, pairs, pair_items, 0)
+    together(mix_steps(last - 2, pairs - 1), exp_steps(last - 1))
+    together(mix_steps(last - 1, pairs - 1))
     start_all(oscatter[pairs - 1])
     for (pair, item) in sorted(events):
         if pair >= pairs:
             for action in events[(pair, item)]:
                 action()
-    for step in range(2, half_count - 1):
-        ring_forward(0, step)
+    ring_forward(0, 0)
+    for pair in range(pairs - 1):
+        ring_forward(4 + pair, 0)
     out_moments(pairs - 1)
-    ring_forward(0, half_count - 1)
+    ring_forward(0, 1)
+    for step in range(half_count):
+        ring_forward(3 + pairs, step)
+        for pair in range(pairs - 1):
+            if step + 1 < half_count:
+                ring_forward(4 + pair, step + 1)
+        if step + 2 < half_count:
+            ring_forward(0, step + 2)
+    for pair in range(pairs - 1):
+        out_arrived(pair)
+        out_step(pair)
     out_copy(3 + 2 * pairs).start()
     out_arrived(pairs - 1)
     out_update()
@@ -495,12 +539,12 @@
         if step < half_count - 1:
             block_copy(owner(place - back)).start()
         block_copy(owner(place + back)).start()
-    for copy in vscatter + vgather + square_copies(0) + square_copies(1):
+    for copy in vscatter + square_copies(0) + square_copies(1):
         copy.wait_send()
     for at in range(pairs):
-        for copy in oscatter[at] + ogather[at]:
+        for copy in oscatter[at]:
             copy.wait_send()
-    for mat in range(3):
+    for mat in range(4 + pairs):
         for step in range(half_count):
             for way in range(2):
                 ring_copy(mat, step, way, False).wait_send()
@@ -635,8 +679,9 @@
             vmem(value_weight), vmem(out_weight), pltpu.VMEM((width, cols), BF16),
             pltpu.VMEM(rest_shape, BF16), pltpu.VMEM(early_shape, F32),
             pltpu.VMEM((2, 8, 128), F32),
-            pltpu.VMEM((seq_len, TILE), F32),
-            pltpu.VMEM((seq_len, TILE), F32),
+            pltpu.VMEM((HELD, 2, seq_len, TILE), F32),
+            pltpu.VMEM((HELD, 2, 8, TILE), F32),
+            pltpu.VMEM((HELD, 2, 8, TILE), F32),
             pltpu.VMEM((seq_len, TILE), BF16),
             pltpu.VMEM((heads, DV, seq_len), BF16),
             pltpu.VMEM((rank, width), BF16),
@@ -656,10 +701,8 @@
             dma((13,)), dma((SLOTS,)),
             dma((fs_count - 1,)), dma((fs_count - 1,)),
             dma((pairs, fs_count - 1)), dma((pairs, fs_count - 1)),
-            dma((fs_count - 1,)), dma((fs_count - 1,)),
-            dma((pairs, fs_count - 1)), dma((pairs, fs_count - 1)),
             dma((2, tp_count - 1)), dma((2, tp_count - 1)),
-            dma((3, 2, half_count)), dma((3, 2, half_count)),
+            dma((4 + pairs, 2, half_count)), dma((4 + pairs, 2, half_count)),
             dma((5 + 2 * pairs,)), dma((fs_count,)),
         ],
         compiler_params=pltpu.CompilerParams(

time: 129 us -> 122 us (0.946)
  Pallas kernels: 128 us -> 121 us
    pallas_call x1, Pallas kernels: 122 us -> 115 us  [body(): pl.pallas_call(functools.partial(step_kernel, fs_count, tp_count), out_sh...]
where the time goes in v3:
time: 122 us
  Pallas kernels  121 us (99%)
    pallas_call x1, Pallas kernels, body(): pl.pallas_call(functools.partial(step_kernel, fs_count, tp_count), out_sh...  115 us
    pallas_call x1, Pallas kernels, body(): pl.pallas_call(finish_kernel, out_shape=results, in_specs=[anywhere] * le...  6.28 us

profile of v3, /device:TPU:0, one launch (start us, length us, event | category | flops | bytes accessed | tf_op | source)
XLA Modules:
  0.0 121.7 jit_solution(16929344490311138742)
XLA Ops:
  0.6 114.6 %step.1 = (f32[32,512]{1,0:T(8,128)}, f32[2,32,256]{2,1,0:T(8,128)}, f32[256,512]{1,0:T(8,128)}, f32[2,256,256]{2,1,0:T(8,128)}, f32[2,8,128]{2,1,0:T(8,128)}, /...) custom-call(f32[4]{0:T(128)} %lam_ref.1, f32[1,128]{1,0:T(1,128)} %bitcast.1, ...), custom_call_target="tpu_custom_call" | custom-call | tf_op jit(solution)/shard_map/step/pallas_call | solution.py:658
  115.2 6.3 %finish.1 = (f32[512,256]{1,0:T(8,128)}, f32[256,512]{1,0:T(8,128)}, f32[512,256]{1,0:T(8,128)}, f32[256,512]{1,0:T(8,128)}, bf16[512,2048]{1,0:T(8,128)(2,1)}, ...) custom-call(f32[2,8,128]{2,1,0:T(8,128)} %get-tuple-element.18.refs_, ...), custom_call_target="tpu_custom_call" | custom-call | tf_op jit(solution)/shard_map/finish/pallas_call | solution.py:727
